TPU v7x, 32 devices: a whole 2x2x4 slice. The times are simulated.
32 devices in a mesh: grp: 2 (over y), sp: 4 (over z), tp: 4 (over x, core).
Axes of the slice: x: 2, y: 2, z: 4, core: 2. Of those that a mesh axis runs over, the one named last changes fastest.
Arguments:
- latent: bfloat16 [4096, 4096], P(('grp', 'sp'), 'tp'), parts along dimension 0, may hold values from -42 to 42
- context: bfloat16 [2048, 4096], P(('grp', 'sp'), 'tp'), parts along dimension 0, may hold values from -42 to 42
- conditions: float32 [4, 4096], P('grp', 'sp'), parts along dimension 0, may hold values from -6 to 6
- mod_weight: bfloat16 [4096, 3, 4096], P('sp', None, 'tp'), may hold values from -0.09375 to 0.09375
- norm_gain: float32 [4096], P('tp'), may hold values from 0.1 to 1.9
- w_query: bfloat16 [4096, 2048], P(None, 'tp'), may hold values from -0.09375 to 0.09375
- w_key: bfloat16 [4096, 2048], P(None, 'tp'), may hold values from -0.09375 to 0.09375
- w_value: bfloat16 [4096, 2048], P(None, 'tp'), may hold values from -0.09375 to 0.09375
- query_gain: float32 [64], replicated, may hold values from 1 to 14
- key_gain: float32 [64], replicated, may hold values from 1 to 14
- lambdas: float32 [16], P('tp'), may hold values from 0.3 to 0.8
- out_gain: float32 [128], replicated, may hold values from 0.1 to 1.9
- w_out: bfloat16 [2048, 4096], P(None, 'tp'), may hold values from -0.125 to 0.125
Outputs:
- updated: bfloat16 [4096, 4096], P(('grp', 'sp'), 'tp'), parts along dimension 0
There are 2 independent parts, one for each index of `grp`. A program takes and returns all parts, laid end to end along the dimension named above; an argument that names none is the same for every part. Nothing has to cross between parts.
All inputs are finite; a program needn't handle non-finite values.
Results may differ from a plain program's by a relative error of at most 0.0076.
Values may be sent and summed in bfloat16 or wider, within the bound.
No kernel may reach another device: no remote copies, remote signals or barrier semaphores. Data moves between devices by JAX's collectives and lax.ppermute only.
A program may use at most 128 MiB of HBM per device.

v0:
```python
import math

import jax
import jax.numpy as jnp
from jax import lax
from jax.sharding import PartitionSpec as P

DK = 64
DV = 128
GRID_W = 64


epsilon = 1e-06


def turn_half(halves, angles):
    quarter = halves.shape[-1] // 2
    cosine = jnp.cos(angles)[:, None, None, :]
    sine_part = jnp.sin(angles)[:, None, None, :]
    first_part = halves[..., :quarter]
    second = halves[..., quarter:]
    return jnp.concatenate(
        [first_part * cosine - second * sine_part, first_part * sine_part + second * cosine],
        axis=-1,
    )


def rotate(features, positions):
    half_width = features.shape[-1] // 2
    quarter = half_width // 2
    inverse = 10000.0 ** (-2.0 * jnp.arange(quarter, dtype=jnp.float32) / half_width)
    grid_row = (positions // GRID_W).astype(jnp.float32)
    grid_column = (positions % GRID_W).astype(jnp.float32)
    return jnp.concatenate(
        [
            turn_half(features[..., :half_width], grid_row[:, None] * inverse),
            turn_half(features[..., half_width:], grid_column[:, None] * inverse),
        ],
        axis=-1,
    )


def head_norm(features, gain_row):
    return (
        features
        * lax.rsqrt(jnp.mean(features * features, axis=-1, keepdims=True) + epsilon)
        * gain_row
    )


def modulate(rows_in, gain_row, shift_row, scale_row):
    floats = rows_in.astype(jnp.float32)
    factor = lax.rsqrt(jnp.mean(floats * floats, axis=1, keepdims=True) + epsilon)
    return (floats * factor * gain_row * (1.0 + scale_row) + shift_row).astype(jnp.bfloat16)


def local(
    latent,
    context,
    conditions,
    mod_weight,
    norm_gain,
    w_query,
    w_key,
    w_value,
    query_gain,
    key_gain,
    lambdas,
    out_gain,
    w_out,
):
    tok_rows = latent.shape[0]
    ctx_rows = context.shape[0]
    columns = latent.shape[1]
    heads_here = lambdas.shape[0]
    in_rows = mod_weight.shape[0]
    activated = jax.nn.silu(conditions).astype(jnp.bfloat16)
    partial_mod = jnp.dot(
        activated, mod_weight.reshape(in_rows, 3 * columns), preferred_element_type=jnp.float32
    ).reshape(2, 3, columns)
    modulation = lax.psum(partial_mod, "sp")
    lat_floats = latent.astype(jnp.float32)
    full_gain, full_pairs = (
        lax.all_gather(norm_gain, "tp", axis=0, tiled=True),
        lax.all_gather(modulation[:, :2], "tp", axis=2, tiled=True),
    )
    whole_lat, whole_ctx = (
        lax.all_gather(latent, "tp", axis=1, tiled=True),
        lax.all_gather(context, "tp", axis=1, tiled=True),
    )
    hidden = modulate(whole_lat, full_gain, full_pairs[0, 0], full_pairs[0, 1])
    hidden_ctx = modulate(whole_ctx, full_gain, full_pairs[1, 0], full_pairs[1, 1])
    query_raw = jnp.dot(hidden, w_query, preferred_element_type=jnp.float32)
    key_raw = jnp.dot(hidden, w_key, preferred_element_type=jnp.float32)
    value_raw = jnp.dot(hidden, w_value, preferred_element_type=jnp.float32)
    ctx_key_raw = jnp.dot(hidden_ctx, w_key, preferred_element_type=jnp.float32)
    ctx_value_raw = jnp.dot(hidden_ctx, w_value, preferred_element_type=jnp.float32)
    positions = lax.axis_index("sp") * tok_rows + jnp.arange(tok_rows, dtype=jnp.int32)
    queries = rotate(
        head_norm(query_raw.reshape(tok_rows, heads_here, 2, DK), query_gain), positions
    ).astype(jnp.bfloat16)
    lat_keys = (
        rotate(head_norm(key_raw.reshape(tok_rows, heads_here, 2, DK), key_gain), positions)
        .astype(jnp.bfloat16)
        .reshape(tok_rows, heads_here * 2 * DK)
    )
    lat_values = value_raw.astype(jnp.bfloat16)
    ctx_keys = (
        head_norm(ctx_key_raw.reshape(ctx_rows, heads_here, 2, DK), key_gain)
        .astype(jnp.bfloat16)
        .reshape(ctx_rows, heads_here * 2 * DK)
    )
    ctx_values = ctx_value_raw.astype(jnp.bfloat16)
    scaling = DK ** (-0.5)

    def absorb(carried, key_rows, value_rows):
        key_count = key_rows.shape[0]
        key_block = key_rows.reshape(key_count, heads_here, 2, DK)
        value_block = value_rows.reshape(key_count, heads_here, DV)
        running_max, totals, weighted = carried
        scores = (
            jnp.einsum("qhmd,khmd->qhmk", queries, key_block, preferred_element_type=jnp.float32)
            * scaling
        )
        new_max = jnp.maximum(running_max, jnp.max(scores, axis=-1))
        rescale = jnp.exp(running_max - new_max)
        exponent = jnp.exp(scores - new_max[..., None])
        totals = totals * rescale + jnp.sum(exponent, axis=-1)
        weighted = weighted * rescale[..., None] + jnp.einsum(
            "qhmk,khv->qhmv",
            exponent.astype(jnp.bfloat16),
            value_block,
            preferred_element_type=jnp.float32,
        )
        return (new_max, totals, weighted)

    def absorb_rows(carried, key_rows, value_rows):
        key_count = key_rows.shape[0]
        block_rows = math.gcd(key_count, 512)

        def visit_block(block_index, partial_value):
            first_row = block_index * block_rows
            return absorb(
                partial_value,
                lax.dynamic_slice_in_dim(key_rows, first_row, block_rows, 0),
                lax.dynamic_slice_in_dim(value_rows, first_row, block_rows, 0),
            )

        return lax.fori_loop(0, key_count // block_rows, visit_block, carried)

    initial_state = (
        jnp.full((tok_rows, heads_here, 2), -1e30, jnp.float32),
        jnp.zeros((tok_rows, heads_here, 2), jnp.float32),
        jnp.zeros((tok_rows, heads_here, 2, DV), jnp.float32),
    )
    every_ctx_keys, every_ctx_values = (
        lax.all_gather(ctx_keys, "sp", axis=0, tiled=True),
        lax.all_gather(ctx_values, "sp", axis=0, tiled=True),
    )
    carried = absorb_rows(initial_state, every_ctx_keys, every_ctx_values)
    carried = absorb_rows(
        carried,
        lax.all_gather(lat_keys, "sp", axis=0, tiled=True),
        lax.all_gather(lat_values, "sp", axis=0, tiled=True),
    )
    running_max, totals, weighted = carried
    attended = (
        weighted[:, :, 0] / totals[:, :, 0, None]
        - lambdas[None, :, None] * weighted[:, :, 1] / totals[:, :, 1, None]
    )
    head_out = head_norm(attended, out_gain).astype(jnp.bfloat16).reshape(tok_rows, heads_here * DV)
    mixed_rows = jnp.dot(
        lax.all_gather(head_out, "tp", axis=1, tiled=True),
        w_out,
        preferred_element_type=jnp.float32,
    )
    return (lat_floats + modulation[0, 2] * mixed_rows).astype(jnp.bfloat16)


def solution(mesh):
    in_specs = (
        P(("grp", "sp"), "tp"),
        P(("grp", "sp"), "tp"),
        P("grp", "sp"),
        P("sp", None, "tp"),
        P("tp"),
        P(None, "tp"),
        P(None, "tp"),
        P(None, "tp"),
        P(),
        P(),
        P("tp"),
        P(),
        P(None, "tp"),
    )
    out_specs = P(("grp", "sp"), "tp")
    return jax.shard_map(local, mesh=mesh, in_specs=in_specs, out_specs=out_specs, check_vma=False)
```

profile of v0, /device:TPU:0, one launch (start us, length us, event | category | flops | bytes accessed | tf_op | source)
XLA Modules:
  0.0 294.6 jit_solution(11514742589361231051)
XLA Ops:
  8.8 8.6 %copy.31 = bf16[1024,3,1024]{0,2,1:T(8,128)(2,1)} copy(bf16[1024,3,1024]{2,0,1:T(8,128)(2,1)} %param.20) | data formatting | bytes 12582912 | tf_op args[3]
  17.5 5.1 %fusion.27 = f32[2,3,1024]{2,0,1:T(2,128)S(1)} fusion(bf16[1024,3,1024]{0,2,1:T(8,128)(2,1)} %copy.31, f32[2,1024]{1,0:T(2,128)S(1)} %copy-done.4), kind=kOutput, calls=%fused_computation.39 | convolution fusion | flops 12593152 | bytes 6324224 | tf_op jit(solution)/shard_map/dot_general | solution.py:78
  22.5 20.6 %psum.7 = f32[2,3,1024]{2,0,1:T(2,128)S(1)} all-reduce(f32[2,3,1024]{2,0,1:T(2,128)S(1)} %fusion.27), channel_id=1, replica_groups=mesh['grp'=2,'sp'=4,'tp'=4] {'sp'}, use_global_device_ids=true, to_apply=%region_0.1 | all-reduce | flops 6144 | bytes 49152 | tf_op jit(solution)/shard_map/psum | solution.py:81
  43.2 5.2 %all_gather.28 = f32[4096]{0:T(1024)S(1)} all-gather(f32[1024]{0:T(1024)S(1)} %copy-done.7), channel_id=1, replica_groups=mesh['grp'=2,'sp'=4,'tp'=4] {'tp'}, dimensions={0}, use_global_device_ids=true | all-gather | bytes 20480 | tf_op jit(solution)/shard_map/all_gather | solution.py:84
  48.4 5.6 %all_gather.29 = f32[2,2,4096]{2,0,1:T(2,128)S(1)} all-gather(f32[2,2,1024]{2,0,1:T(2,128)S(1)} %slice.85), channel_id=1, replica_groups=mesh['grp'=2,'sp'=4,'tp'=4] {'tp'}, dimensions={2}, use_global_device_ids=true | all-gather | bytes 81920 | tf_op jit(solution)/shard_map/all_gather | solution.py:85
  54.1 2.1 fusion.29
  56.2 4.9 %convolution_convert_fusion.1 = bf16[256,512]{1,0:T(8,128)(2,1)} fusion(bf16[4096,512]{1,0:T(8,128)(2,1)} %param.24, bf16[256,4096]{1,0:T(8,128)(2,1)} %all-gather.8.cloned.1.call-done, f32[4096]{0:T(1024)S(1)} %bitcast.202, f32[4096]{0:T(1024)S(1)} %bitcast.204, f32[4096]{0:T(1024)S(1)} %all_gather.28, f32[256]{0:T(256)S(1)} %add_rsqrt_fusion.5), kind=kOutput, calls=%fused_computation.50 | convolution fusion | flops 1080164352 | bytes 6603776 | tf_op jit(solution)/shard_map/dot_general | solution.py:97
  61.4 5.0 %fusion.59 = (f32[256,512]{1,0:T(8,128)S(1)}, f32[256,512]{1,0:T(8,128)}) fusion(bf16[4096,512]{1,0:T(8,128)(2,1)} %param.23, bf16[256,4096]{1,0:T(8,128)(2,1)} %all-gather.8.cloned.1.call-done, f32[4096]{0:T(1024)S(1)} %bitcast.203, f32[4096]{0:T(1024)S(1)} %bitcast.205, f32[4096]{0:T(1024)S(1)} %all_gather.28, f32[256]{0:T(256)S(1)} %add_rsqrt_fusion.5), kind=kOutput, calls=%fused_computation.117 | convolution fusion | flops 1080164352 | bytes 7390208 | tf_op jit(solution)/shard_map/dot_general | solution.py:96
  70.7 3.2 %fusion.22 = f32[512]{0:T(512)S(1)} fusion(bf16[512,4096]{1,0:T(8,128)(2,1)} %all-gather.12.cloned.1.call-done), kind=kLoop, calls=%fused_computation.34 | loop fusion | flops 6290944 | bytes 4196352 | tf_op jit(solution)/shard_map/reduce_sum | solution.py:53
  74.1 5.4 %convolution_convert_fusion = bf16[512,512]{1,0:T(8,128)(2,1)} fusion(bf16[4096,512]{1,0:T(8,128)(2,1)} %param.24, bf16[512,4096]{1,0:T(8,128)(2,1)S(1)} %copy-done, f32[4096]{0:T(1024)S(1)} %bitcast.199, f32[4096]{0:T(1024)S(1)} %bitcast.196, f32[4096]{0:T(1024)S(1)} %all_gather.28, f32[512]{0:T(512)S(1)} %add_rsqrt_fusion.4), kind=kOutput, calls=%fused_computation.49 | convolution fusion | flops 2160328704 | bytes 8964096 | tf_op jit(solution)/shard_map/dot_general | solution.py:95
  79.8 6.4 %multiply_reduce_fusion = (f32[512,4,2]{0,2,1:T(2,128)S(1)}, f32[512,512]{0,1:T(8,128)S(1)}) fusion(bf16[4096,512]{1,0:T(8,128)(2,1)} %param.23, bf16[512,4096]{1,0:T(8,128)(2,1)} %all-gather.12.cloned.1.call-done, f32[4096]{0:T(1024)S(1)} %bitcast.200, f32[4096]{0:T(1024)S(1)} %bitcast.197, f32[4096]{0:T(1024)S(1)} %all_gather.28, f32[512]{0:T(512)S(1)} %add_rsqrt_fusion.4), kind=kOutput, calls=%fused_computation.64 | convolution fusion | flops 2160586752 | bytes 9504768 | tf_op jit(solution)/shard_map/dot_general | solution.py:94
  88.6 2.8 multiply_reduce_fusion.1
  92.2 8.0 %all-gather.14.cloned.1.call-done = bf16[1024,512]{1,0:T(8,128)(2,1)} async-done(((bf16[256,512]{1,0:T(8,128)(2,1)}), bf16[1024,512]{1,0:T(8,128)(2,1)}) %all-gather.14.cloned.1.call-update) | async-done | bytes 1048592 | tf_op jit(solution)/shard_map/all_gather | solution.py:158
  100.2 28.8 %all-gather.10.cloned.1.call-done = bf16[1024,512]{1,0:T(8,128)(2,1)} async-done(((bf16[256,512]{1,0:T(8,128)(2,1)}), bf16[1024,512]{1,0:T(8,128)(2,1)}) %all-gather.10.cloned.1.call-update) | async-done | bytes 1048592 | tf_op jit(solution)/shard_map/all_gather | solution.py:157
  129.0 20.6 %while.36 = (s32[]{:T(128)}, f32[512,4,2]{0,2,1:T(2,128)S(1)}, f32[512,4,2]{0,2,1:T(2,128)S(1)}, f32[512,4,2,128]{0,3,2,1:T(8,128)S(1)}, bf16[1024,512]{1,0:T(8,...) while((s32[]{:T(128)}, f32[512,4,2]{0,2,1:T(2,128)S(1)}, ...), condition=%wide.region_8.9_spmd.clone, body=%wide.region_5.8_spmd.clone.sunk | while | flops 823676928 | bytes 35389616 | solution.py:149
  129.0 2.1 constant_dynamic-slice_fusion.9
  133.3 2.4 bitcast_reduce_fusion.6
  137.2 2.1 bitcast_add_fusion.5
  139.3 2.1 constant_dynamic-slice_fusion.9
  143.7 2.4 bitcast_reduce_fusion.6
  147.5 2.1 bitcast_add_fusion.5
  149.7 25.8 %all-gather.18.cloned.1.call-done = bf16[2048,512]{1,0:T(8,128)(2,1)} async-done(((bf16[512,512]{1,0:T(8,128)(2,1)}), bf16[2048,512]{1,0:T(8,128)(2,1)}) %all-gather.18.cloned.1.call-update) | async-done | bytes 2097168 | tf_op jit(solution)/shard_map/all_gather | solution.py:164
  175.5 45.9 %all-gather.16.cloned.1.call-done = bf16[2048,512]{0,1:T(8,128)(2,1)} async-done(((bf16[512,512]{0,1:T(8,128)(2,1)}), bf16[2048,512]{0,1:T(8,128)(2,1)}) %all-gather.16.cloned.1.call-update) | async-done | bytes 2097168 | tf_op jit(solution)/shard_map/all_gather | solution.py:163
  221.4 36.4 %while.35 = (s32[]{:T(128)}, f32[512,4,2]{0,2,1:T(2,128)S(1)}, f32[512,4,2]{0,2,1:T(2,128)S(1)}, f32[512,4,2,128]{0,3,2,1:T(8,128)S(1)}, bf16[2048,512]{0,1:T(8,...) while((s32[]{:T(128)}, f32[512,4,2]{0,2,1:T(2,128)S(1)}, ...), condition=%wide.region_13.14_spmd, body=%wide.region_10.13_spmd.sunk | while | flops 823140352 | bytes 34341024 | solution.py:149
  228.4 2.1 bitcast_add_fusion.4
  230.5 1.9 constant_dynamic-slice_fusion.8
  237.5 2.1 bitcast_add_fusion.4
  239.6 1.9 constant_dynamic-slice_fusion.8
  246.6 2.1 bitcast_add_fusion.4
  255.7 2.1 bitcast_add_fusion.4
  260.8 20.8 %all-gather.20.cloned.1.call-done = bf16[512,2048]{0,1:T(8,128)(2,1)} async-done(((bf16[512,512]{0,1:T(8,128)(2,1)}), bf16[512,2048]{0,1:T(8,128)(2,1)}) %all-gather.20.cloned.1.call-update) | async-done | bytes 2097168 | tf_op jit(solution)/shard_map/all_gather | solution.py:173
  281.6 6.1 %add_convert_fusion = bf16[512,1024]{1,0:T(8,128)(2,1)} fusion(bf16[512,1024]{1,0:T(8,128)(2,1)S(1)} %copy-done.2, bf16[512,2048]{0,1:T(8,128)(2,1)} %all-gather.20.cloned.1.call-done, bf16[2048,1024]{1,0:T(8,128)(2,1)} %param.29, f32[1024]{0:T(1024)S(1)} %bitcast.206), kind=kOutput, calls=%fused_computation.48 | convolution fusion | flops 2149580800 | bytes 8392704 | tf_op jit(solution)/shard_map/dot_general | solution.py:172
  (123 shorter events, 44.9 us)
Async XLA Ops:
  6.5 47.5 %all-gather.8.cloned.1.call-start = ((), (), s32[]{:S(2)}) async-start(), calls=%async_computation | async-start | bytes 2621440 | tf_op jit(solution)/shard_map/all_gather | solution.py:89
  7.3 63.4 %all-gather.12.cloned.1.call-start = ((), (), s32[]{:S(2)}) async-start(), calls=%async_computation.2 | async-start | bytes 5242880 | tf_op jit(solution)/shard_map/all_gather | solution.py:88
  8.0 92.2 %all-gather.14.cloned.1.call-start = ((), (), s32[]{:S(2)}) async-start(), calls=%async_computation.3 | async-start | bytes 1310720 | tf_op jit(solution)/shard_map/all_gather | solution.py:158
  8.8 8.7 %copy-start.4 = (f32[2,1024]{1,0:T(2,128)S(1)}, f32[2,1024]{1,0:T(2,128)}, u32[]{:S(2)}) copy-start(f32[2,1024]{1,0:T(2,128)} %param.19) | copy-start | bytes 24580
  17.5 25.7 %copy-start.7 = (f32[1024]{0:T(1024)S(1)}, f32[1024]{0:T(1024)}, u32[]{:S(2)}) copy-start(f32[1024]{0:T(1024)} %param.21) | copy-start | bytes 12292
  43.1 17.9 %copy-start.3 = (f32[2,3,1024]{2,0,1:T(2,128)}, f32[2,3,1024]{2,0,1:T(2,128)S(1)}, u32[]{:S(2)}) copy-start(f32[2,3,1024]{2,0,1:T(2,128)S(1)} %psum.7) | copy-start | bytes 73732
  61.0 68.0 %all-gather.10.cloned.1.call-start = ((), (), s32[]{:S(2)}) async-start(), calls=%async_computation.1 | async-start | bytes 1310720 | tf_op jit(solution)/shard_map/all_gather | solution.py:157
  66.4 2.5 copy-start.9
  66.4 2.5 copy-start.12
  68.8 106.7 %all-gather.18.cloned.1.call-start = ((), (), s32[]{:S(2)}) async-start(), calls=%async_computation.5 | async-start | bytes 2621440 | tf_op jit(solution)/shard_map/all_gather | solution.py:164
  70.7 3.4 %copy-start = (bf16[512,4096]{1,0:T(8,128)(2,1)S(1)}, bf16[512,4096]{1,0:T(8,128)(2,1)}, u32[]{:S(2)}) copy-start(bf16[512,4096]{1,0:T(8,128)(2,1)} %all-gather.12.cloned.1.call-done) | copy-start | bytes 12582916
  79.5 6.7 %copy-start.8 = (f32[64]{0:T(128)S(1)}, f32[64]{0:T(128)}, u32[]{:S(2)}) copy-start(f32[64]{0:T(128)} %param.26) | copy-start | bytes 772
  79.5 141.9 %all-gather.16.cloned.1.call-start = ((), (), s32[]{:S(2)}) async-start(), calls=%async_computation.4 | async-start | bytes 2621440 | tf_op jit(solution)/shard_map/all_gather | solution.py:163
  79.8 7.7 %copy-start.13 = (bf16[4096,512]{1,0:T(8,128)(2,1)S(1)}, bf16[4096,512]{1,0:T(8,128)(2,1)}, u32[]{:S(2)}) copy-start(bf16[4096,512]{1,0:T(8,128)(2,1)} %param.22) | copy-start | bytes 12582916
  86.2 2.4 copy-start.1
  88.6 2.8 copy-start.11
  91.9 189.7 %all-gather.20.cloned.1.call-start = ((), (), s32[]{:S(2)}) async-start(), calls=%async_computation.6 | async-start | bytes 2621440 | tf_op jit(solution)/shard_map/all_gather | solution.py:173
  257.9 0.7 copy-start.10
  258.0 1.0 copy-start.5
  258.0 1.0 copy-start.6
  258.2 23.4 %copy-start.2 = (bf16[512,1024]{1,0:T(8,128)(2,1)S(1)}, bf16[512,1024]{1,0:T(8,128)(2,1)}, u32[]{:S(2)}) copy-start(bf16[512,1024]{1,0:T(8,128)(2,1)} %param.17) | copy-start | bytes 3145732
Sparse Core Ops, SparseCore 0:
  8.9 25.2 all-gather.7
  35.8 34.8 all-gather.11
  72.3 27.8 all-gather.13
  101.6 27.3 all-gather.9
  130.4 45.0 all-gather.17
  176.9 44.4 all-gather.15
  260.2 21.3 all-gather.19
where the time goes:
time: 296 us; the launch traced here: 295 us
  waiting for transfers between devices  132 us (45%)
  matrix products  58.2 us (20%)
  local copies, waits for them, and re-layouts  38.6 us (13%)
  blocking collectives  31.4 us (11%)
  other arithmetic  19.5 us (7%)
  between operations  13.9 us (5%)
    all_gather x1, waiting for transfers between devices, local(): lax.all_gather(lat_keys, 'sp', axis=0, tiled=True)  45.9 us
    all_gather x1, waiting for transfers between devices, local(): lax.all_gather(ctx_keys, 'sp', axis=0, tiled=True)  28.8 us
    all_gather x1, waiting for transfers between devices, local(): lax.all_gather(lat_values, 'sp', axis=0, tiled=True)  25.8 us
    all_gather x1, waiting for transfers between devices, local(): lax.all_gather(head_out, 'tp', axis=1, tiled=True)  20.8 us
    psum x1, blocking collectives, local(): modulation = lax.psum(partial_mod, 'sp')  20.6 us
    dynamic_slice x12, local copies, waits for them, and re-layouts, visit_block(): lax.dynamic_slice_in_dim(value_rows, first_row, block_rows, 0)  19.1 us
    dot_general x6, matrix products, absorb(): jnp.einsum('qhmk,khv->qhmv', exponent.astype(jnp.bfloat16), value_block,...  12.7 us
    unnamed x31, local copies, waits for them, and re-layouts  10.2 us
  transfers between devices with their start and end apart: 7, of which 6 were waited for; matrix products, arithmetic and copies ran while one was open for 24% of the time, Pallas kernels for 0%

commit v1 on v0

v1 whole, which is shorter than its diff:
```python
import functools

import jax
import jax.numpy as jnp
from jax import lax
from jax.experimental import pallas as pl
from jax.experimental.pallas import tpu as pltpu
from jax.sharding import PartitionSpec as P

GRID_W = 64
EPS = 1e-06
F32 = jnp.float32
BF16 = jnp.bfloat16
VMEM_LIMIT = 60 * 1024 * 1024


def tables(positions, dk):
    half, quarter = dk // 2, dk // 4
    lane = jnp.arange(2 * dk, dtype=jnp.int32) % dk
    inverse = 10000.0 ** (-2.0 * (lane % quarter).astype(F32) / half)
    grid_row = (positions // GRID_W).astype(F32)[:, None]
    grid_column = (positions % GRID_W).astype(F32)[:, None]
    angles = jnp.where(lane[None] < half, grid_row, grid_column) * inverse[None]
    sign = jnp.where(lane % half < quarter, -1.0, 1.0).astype(F32)
    return jnp.cos(angles), jnp.sin(angles) * sign[None]


def project_kernel(order, my_ref, other_ref, mods_ref, *refs, parts, weights, turned, features):
    w_refs = [refs[i * parts : (i + 1) * parts] for i in range(weights)]
    refs = refs[weights * parts :]
    gain_refs, refs = refs[: weights - 1], refs[weights - 1 :]
    if turned:
        cos_ref, sin_ref = refs[:2]
        refs = refs[2:]
    out_ref, hidden = refs
    half_parts = parts // 2

    @pl.when(pl.program_id(0) == 0)
    def _():
        total = None
        for b in range(parts):
            src = my_ref if b < half_parts else other_ref
            rows = src[b % half_parts].astype(F32)
            part = jnp.sum(rows * rows, axis=-1, keepdims=True)
            total = part if total is None else total + part
        factor = lax.rsqrt(total / features + EPS)
        for b in range(parts):
            src = my_ref if b < half_parts else other_ref
            rows = src[b % half_parts].astype(F32)
            gain = mods_ref[b, 0:1, :] * (1.0 + mods_ref[b, 1:2, :])
            hidden[b] = (rows * factor * gain + mods_ref[b, 2:3, :]).astype(BF16)

    def product(w):
        total = None
        for b in range(parts):
            part = jnp.dot(hidden[b], w_refs[w][b][...], preferred_element_type=F32)
            total = part if total is None else total + part
        return total

    heads, rows, width = out_ref.shape
    dv = width // weights
    dk = dv // 2
    lane = lax.broadcasted_iota(jnp.int32, (rows, dv), 1)
    low = lane < dk
    first = lane % (dk // 2) < dk // 4
    for w in range(weights):
        raw = product(w)
        for h in range(heads):
            v = raw[:, h * dv : (h + 1) * dv]
            if w < weights - 1:
                sq = v * v
                low_sum = jnp.sum(jnp.where(low, sq, 0.0), axis=-1, keepdims=True)
                high_sum = jnp.sum(jnp.where(low, 0.0, sq), axis=-1, keepdims=True)
                mean = jnp.where(low, low_sum, high_sum) / dk
                v = v * lax.rsqrt(mean + EPS) * gain_refs[w][...]
                if turned:
                    swapped = jnp.where(
                        first, pltpu.roll(v, dv - dk // 4, 1), pltpu.roll(v, dk // 4, 1)
                    )
                    v = v * cos_ref[...] + swapped * sin_ref[...]
            out_ref[h, :, w * dv : (w + 1) * dv] = v.astype(BF16)


def project(order, my, other, mods, w_list, gains, cos_sin, dv):
    half_parts, rows, width = my.shape
    parts = 2 * half_parts
    cols = w_list[0].shape[1]
    block = min(cols, 2 * dv)
    weights = len(w_list)
    full = lambda shape: pl.BlockSpec(shape, lambda j, order: (0,) * len(shape))
    in_specs = [full(my.shape), full(other.shape), full(mods.shape)]
    operands = [my, other, mods]
    for w in w_list:
        for b in range(parts):
            in_specs.append(pl.BlockSpec((width, block), lambda j, order, b=b: (order[b], j)))
            operands.append(w)
    for extra in list(gains) + list(cos_sin):
        in_specs.append(full(extra.shape))
        operands.append(extra)
    return pl.pallas_call(
        functools.partial(
            project_kernel,
            parts=parts,
            weights=weights,
            turned=bool(cos_sin),
            features=float(parts * width),
        ),
        grid_spec=pltpu.PrefetchScalarGridSpec(
            num_scalar_prefetch=1,
            grid=(cols // block,),
            in_specs=in_specs,
            out_specs=pl.BlockSpec((block // dv, rows, weights * dv), lambda j, order: (j, 0, 0)),
            scratch_shapes=[pltpu.VMEM((parts, rows, width), BF16)],
        ),
        out_shape=jax.ShapeDtypeStruct((cols // dv, rows, weights * dv), BF16),
        compiler_params=pltpu.CompilerParams(vmem_limit_bytes=VMEM_LIMIT),
        cost_estimate=pl.CostEstimate(
            flops=2 * rows * parts * width * cols * weights,
            transcendentals=0,
            bytes_accessed=2 * parts * width * cols * weights,
        ),
    )(order, *operands)


def attend_kernel(lam_ref, *refs, scaling, step, pairs, resumed, final, after):
    q_ref, refs = refs[0], refs[1:]
    key_refs, refs = [refs[2 * i : 2 * i + 2] for i in range(pairs)], refs[2 * pairs :]
    gain_ref, refs = refs[0], refs[1:]
    if resumed:
        old_refs, refs = refs[:3], refs[3:]
    outs = refs[after:]
    q = q_ref[0]
    rows, dv = q.shape
    lane = lax.broadcasted_iota(jnp.int32, (rows, dv), 1)
    zero = jnp.zeros_like(q)
    both = jnp.concatenate(
        [jnp.where(lane < dv // 2, q, zero), jnp.where(lane < dv // 2, zero, q)], axis=0
    )
    pieces = []
    for k_ref, v_ref in key_refs:
        count = k_ref.shape[1]
        size = min(count, step)
        pieces += [(k_ref, v_ref, start, size) for start in range(0, count, size)]

    def fold(x, combine, whole, so_far):
        for c in range(0, x.shape[1], 128):
            part = x[:, c : c + 128]
            if part.shape[1] < 128:
                part = jnp.pad(part, ((0, 0), (0, 128 - part.shape[1])), constant_values=whole)
            so_far = part if so_far is None else combine(so_far, part)
        return so_far

    scores = []
    peak = None
    for k_ref, _, start, size in pieces:
        s = lax.dot_general(
            both, k_ref[0, start : start + size, :], (((1,), (1,)), ((), ())),
            preferred_element_type=F32,
        )
        scores.append(s)
        peak = fold(s, jnp.maximum, -jnp.inf, peak)
    factor = scaling * 1.4426950408889634
    peak = jnp.max(peak, axis=-1, keepdims=True) * factor
    if resumed:
        old_peak = old_refs[1][0][:, :1]
        peak = jnp.maximum(peak, old_peak)
    sums = None
    blended = None
    for (_, v_ref, start, size), s in zip(pieces, scores):
        expo = jnp.exp2(s * factor - peak)
        sums = fold(expo, jnp.add, 0.0, sums)
        more = jnp.dot(
            expo.astype(BF16), v_ref[0, start : start + size, :], preferred_element_type=F32
        )
        blended = more if blended is None else blended + more
    sums = jnp.sum(sums, axis=-1, keepdims=True)
    if resumed:
        shrink = jnp.exp2(old_peak - peak)
        blended = blended + old_refs[0][0] * shrink
        sums = sums + old_refs[2][0][:, :1] * shrink
    if not final:
        outs[0][0] = blended
        outs[1][0] = jnp.broadcast_to(peak, (2 * rows, 128))
        outs[2][0] = jnp.broadcast_to(sums, (2 * rows, 128))
        return
    normed = blended / sums
    attended = normed[:rows] - lam_ref[pl.program_id(0)] * normed[rows:]
    mean = jnp.mean(attended * attended, axis=-1, keepdims=True)
    outs[0][0] = (attended * lax.rsqrt(mean + EPS) * gain_ref[...]).astype(BF16)


def attend(lam, q, q_at, keys, gain, dv, state=(), final=True, after=(), share=(0, 1)):
    heads, count = q.shape[0], q.shape[1] // share[1]
    total = sum(x.shape[1] for x, _ in keys)
    rows = min(count, 256 if total <= 4096 else 128)
    first = share[0] * (count // rows)
    spec = lambda n, at: pl.BlockSpec((1, n, dv), lambda h, i: (h, 0, at))
    kept = lambda width: pl.BlockSpec((1, 2 * rows, width), lambda h, i: (h, i, 0))
    in_specs = [
        pl.BlockSpec(memory_space=pltpu.SMEM),
        pl.BlockSpec((1, rows, dv), lambda h, i: (h, first + i, q_at)),
    ]
    operands = [lam, q]
    for x, at in keys:
        in_specs += [spec(x.shape[1], at), spec(x.shape[1], at + 1)]
        operands += [x, x]
    in_specs.append(pl.BlockSpec((1, dv), lambda h, i: (0, 0)))
    operands.append(gain)
    for x in state:
        in_specs.append(kept(x.shape[2]))
        operands.append(x)
    for x in after:
        in_specs.append(pl.BlockSpec(memory_space=pl.ANY))
        operands.append(x)
    if final:
        out_specs = pl.BlockSpec((1, rows, dv), lambda h, i: (h, i, 0))
        out_shape = jax.ShapeDtypeStruct((heads, count, dv), BF16)
    else:
        out_specs = [kept(dv), kept(128), kept(128)]
        out_shape = [
            jax.ShapeDtypeStruct((heads, 2 * count, width), F32) for width in (dv, 128, 128)
        ]
    return pl.pallas_call(
        functools.partial(
            attend_kernel, scaling=(dv // 2) ** -0.5, step=512, pairs=len(keys),
            resumed=bool(state), final=final, after=len(after),
        ),
        grid=(heads, count // rows),
        in_specs=in_specs,
        out_specs=out_specs,
        out_shape=out_shape,
        compiler_params=pltpu.CompilerParams(vmem_limit_bytes=VMEM_LIMIT),
        cost_estimate=pl.CostEstimate(
            flops=12 * heads * count * total * dv,
            transcendentals=2 * heads * count * total,
            bytes_accessed=4 * heads * total * dv,
        ),
    )(*operands)


def mix_kernel(order, my_ref, other_ref, lat_ref, gate_ref, *refs, parts):
    out_ref = refs[parts]
    half_parts = parts // 2
    total = None
    for b in range(parts):
        src = my_ref if b < half_parts else other_ref
        part = jnp.dot(src[b % half_parts], refs[b][...], preferred_element_type=F32)
        total = part if total is None else total + part
    out_ref[...] = (lat_ref[...].astype(F32) + gate_ref[...] * total).astype(BF16)


def mix(order, my, other, latent, gate, w_out):
    half_parts, rows, width = my.shape
    parts = 2 * half_parts
    cols = w_out.shape[1]
    block = min(cols, 256)
    full = lambda shape: pl.BlockSpec(shape, lambda j, order: (0,) * len(shape))
    return pl.pallas_call(
        functools.partial(mix_kernel, parts=parts),
        grid_spec=pltpu.PrefetchScalarGridSpec(
            num_scalar_prefetch=1,
            grid=(cols // block,),
            in_specs=[
                full(my.shape),
                full(other.shape),
                pl.BlockSpec((rows, block), lambda j, order: (0, j)),
                pl.BlockSpec((1, block), lambda j, order: (0, j)),
            ]
            + [
                pl.BlockSpec((width, block), lambda j, order, b=b: (order[b], j))
                for b in range(parts)
            ],
            out_specs=pl.BlockSpec((rows, block), lambda j, order: (0, j)),
        ),
        out_shape=jax.ShapeDtypeStruct((rows, cols), BF16),
        compiler_params=pltpu.CompilerParams(vmem_limit_bytes=VMEM_LIMIT),
    )(order, my, other, latent, gate, *([w_out] * parts))


def local(
    latent, context, conditions, mod_weight, norm_gain, w_query, w_key, w_value,
    query_gain, key_gain, lambdas, out_gain, w_out, *, n_sp, n_tp,
):
    tok_rows, _ = latent.shape
    heads_here = lambdas.shape[0]
    dk, dv = query_gain.shape[0], out_gain.shape[0]
    sp, tp = lax.axis_index("sp"), lax.axis_index("tp")
    chips = n_tp // 2

    def across(x):
        pieces = [x] + [
            lax.ppermute(x, "tp", [(i, (i + 2 * k) % n_tp) for i in range(n_tp)])
            for k in range(1, chips)
        ]
        return jnp.stack(pieces)

    def partner(x):
        return lax.ppermute(x, "tp", [(i, i ^ 1) for i in range(n_tp)])

    def shift(x, k):
        return lax.ppermute(x, "sp", [(i, (i + k) % n_sp) for i in range(n_sp)])

    places = jnp.arange(chips, dtype=jnp.int32)
    chip_order = (tp // 2 - places) % chips
    order = jnp.concatenate([2 * chip_order + tp % 2, 2 * chip_order + 1 - tp % 2])

    my_ctx = across(context)
    activated = jax.nn.silu(conditions).astype(BF16)
    modulation = jnp.stack(
        [
            jnp.sum(row[:, None, None] * mod_weight.astype(F32), axis=0)
            for row in activated.astype(F32)
        ]
    )
    if n_sp > 4:
        modulation = lax.psum(modulation, "sp")
    else:
        modulation = sum([shift(modulation, k) for k in range(1, n_sp)], modulation)
    gate = modulation[0, 2][None]
    packed = jnp.concatenate(
        [norm_gain[None], modulation[0, 1:2], modulation[0, 0:1],
         norm_gain[None], modulation[1, 1:2], modulation[1, 0:1]], axis=0
    )
    my_mods = across(packed)
    mods = jnp.concatenate([my_mods, partner(my_mods)])
    other_ctx = partner(my_ctx)

    pair = lambda g: jnp.concatenate([g, g])[None]
    ctx = project(
        order, my_ctx, other_ctx, mods[:, 3:], [w_key, w_value], [pair(key_gain)], (), dv
    )
    chunks = 2 if tok_rows % 16 == 0 else 1
    rows = tok_rows // chunks
    exchange = heads_here % n_sp == 0
    per = heads_here // n_sp if exchange else heads_here

    def swap(x):
        at = lambda k: lax.dynamic_slice_in_dim(x, (sp + k) % n_sp * per, per, 0)
        return [at(0)] + [shift(at(k), k) for k in range(1, n_sp)]

    lats = []
    for c in range(chunks):
        my = across(latent[c * rows : (c + 1) * rows])
        other = partner(my)
        positions = sp * tok_rows + c * rows + jnp.arange(rows, dtype=jnp.int32)
        lats.append(
            project(
                order, my, other, mods[:, :3], [w_query, w_key, w_value],
                [pair(query_gain), pair(key_gain)], tables(positions, dk), dv,
            )
        )
    gain = out_gain[None]
    if exchange:
        every_ctx = jnp.concatenate(swap(ctx), axis=1)
        every_lat = [jnp.concatenate(swap(x), axis=1) for x in lats]
        lam = lax.dynamic_slice_in_dim(lambdas, sp * per, per, 0)
        outs = []
        for c in range(chunks):
            seen = [(every_ctx, 0)] + [(x, 1) for x in every_lat[: c + 1]]
            rest = [(x, 1) for x in every_lat[c + 1 :]]
            before = tuple(outs[-1][-1:]) if outs else ()
            if rest:
                state = attend(lam, every_lat[c], 0, seen, gain, dv, final=False, after=before)
                outs.append([attend(lam, every_lat[c], 0, rest, gain, dv, state=state)])
                continue
            outs.append([])
            splits = 1
            for i in range(splits):
                out = attend(lam, every_lat[c], 0, seen, gain, dv, after=before, share=(i, splits))
                outs[-1].append(out)
                before = (out,)
    else:
        every_ctx = lax.all_gather(ctx, "sp", axis=1, tiled=True)
        lat = jnp.concatenate(lats, axis=1)
        every_lat = lax.all_gather(lat[:, :, dv:], "sp", axis=1, tiled=True)
        outs = [
            [attend(lambdas, x, 0, [(every_ctx, 0), (every_lat, 0)], gain, dv)] for x in lats
        ]
    head_out = []
    for out in outs:
        if exchange:
            split = n_sp // len(out)
            blocks = [
                out[k // split][:, k % split * rows : (k % split + 1) * rows] for k in range(n_sp)
            ]
            back = [shift(x, n_sp - k) if k else x for k, x in enumerate(blocks)]
            stacked = jnp.stack(back)
            ordered = [
                lax.dynamic_index_in_dim(stacked, (p - sp) % n_sp, 0, False)[h]
                for p in range(n_sp)
                for h in range(per)
            ]
        else:
            ordered = [out[0][h] for h in range(heads_here)]
        head_out.append(jnp.concatenate(ordered, axis=1))
    my_out = across(jnp.concatenate(head_out))
    return mix(order, my_out, partner(my_out), latent, gate, w_out)


def solution(mesh):
    in_specs = (
        P(("grp", "sp"), "tp"),
        P(("grp", "sp"), "tp"),
        P("grp", "sp"),
        P("sp", None, "tp"),
        P("tp"),
        P(None, "tp"),
        P(None, "tp"),
        P(None, "tp"),
        P(),
        P(),
        P("tp"),
        P(),
        P(None, "tp"),
    )

    def body(*args):
        return local(*args, n_sp=mesh.shape["sp"], n_tp=mesh.shape["tp"])

    return jax.shard_map(
        body, mesh=mesh, in_specs=in_specs, out_specs=P(("grp", "sp"), "tp"), check_vma=False
    )
```

time: 296 us -> 188 us (0.64)
  waiting for transfers between devices: 132 us -> 38 us
  Pallas kernels: 0 us -> 81.3 us
  matrix products: 58.2 us -> 0 us
  starting transfers between devices: 0.65 us -> 42.4 us
  blocking collectives: 31.4 us -> 0 us
  local copies, waits for them, and re-layouts: 38.6 us -> 8.95 us
  between operations: 13.9 us -> 0.38 us
  other arithmetic: 19.5 us -> 16.2 us
    all_gather x7 -> x0, waiting for transfers between devices: 131 us -> none  [the longest x1 45.9 us: local(): lax.all_gather(lat_keys, 'sp', axis=0, tiled=True)]
    pallas_call x0 -> x7, Pallas kernels: none -> 81.3 us  [the longest x3 44.2 us: attend(): pl.pallas_call(functools.partial(attend_kernel, scaling=(dv // 2) ** (-0....]
    dot_general x19 -> x0, matrix products: 58.2 us -> none  [the longest x6 12.7 us: absorb(): jnp.einsum('qhmk,khv->qhmv', exponent.astype(jnp.bfloat16), value_block,...]
    ppermute x0 -> x28, starting transfers between devices: none -> 42.4 us  [the longest x18 35 us: shift(): return lax.ppermute(x, 'sp', [(i, (i + k) % n_sp) for i in range(n_sp)])]
    ppermute x0 -> x28, waiting for transfers between devices: none -> 38 us  [the longest x5 29.8 us: across(): lax.ppermute(x, 'tp', [(i, (i + 2 * k) % n_tp) for i in range(n_tp)])]
    dynamic_slice x18 -> x4, local copies, waits for them, and re-layouts: 25.5 us -> 4.3 us  [the longest x3 3.75 us: swap(): at = lambda k: lax.dynamic_slice_in_dim(x, (sp + k) % n_sp * per, per, 0)]
    psum x1 -> x0, blocking collectives: 20.6 us -> none  [local(): modulation = lax.psum(partial_mod, 'sp')]
    all_gather x2 -> x0, blocking collectives: 10.8 us -> none  [the longest x1 5.6 us: local(): lax.all_gather(modulation[:, :2], 'tp', axis=2, tiled=True)]
  transfers between devices with their start and end apart: 7 -> 28, of which waited for: 6 -> 8; matrix products, arithmetic and copies ran while one was open for 24% -> 9% of each run, Pallas kernels for 0% -> 23%
where the time goes in v1:
time: 188 us; the launch traced here: 187 us
  Pallas kernels  81.3 us (43%)
  starting transfers between devices  42.4 us (23%)
  waiting for transfers between devices  38 us (20%)
  other arithmetic  16.2 us (9%)
  local copies, waits for them, and re-layouts  8.95 us (5%)
    pallas_call x3, Pallas kernels, attend(): pl.pallas_call(functools.partial(attend_kernel, scaling=(dv // 2) ** (-0....  44.2 us
    ppermute x18, starting transfers between devices, shift(): return lax.ppermute(x, 'sp', [(i, (i + k) % n_sp) for i in range(n_sp)])  35 us
    ppermute x5, waiting for transfers between devices, across(): lax.ppermute(x, 'tp', [(i, (i + 2 * k) % n_tp) for i in range(n_tp)])  29.8 us
    pallas_call x3, Pallas kernels, project(): pl.pallas_call(functools.partial(project_kernel, parts=parts, weights=wei...  29.8 us
    pallas_call x1, Pallas kernels, mix(): pl.pallas_call(functools.partial(mix_kernel, parts=parts), grid_spec=pltp...  7.27 us
    ppermute x5, starting transfers between devices, across(): lax.ppermute(x, 'tp', [(i, (i + 2 * k) % n_tp) for i in range(n_tp)])  6.62 us
    ppermute x18, waiting for transfers between devices, shift(): return lax.ppermute(x, 'sp', [(i, (i + k) % n_sp) for i in range(n_sp)])  5.58 us
    reduce_sum x1, other arithmetic, local(): jnp.sum(row[:, None, None] * mod_weight.astype(F32), axis=0)  5.05 us
  transfers between devices with their start and end apart: 28, of which 8 were waited for; matrix products, arithmetic and copies ran while one was open for 9% of the time, Pallas kernels for 23%

profile of v1, /device:TPU:0, one launch (start us, length us, event | category | flops | bytes accessed | tf_op | source)
XLA Modules:
  0.0 187.2 jit_solution(1689940353883282822)
XLA Ops:
  0.8 5.0 %fusion = (f32[3,1024]{1,0:T(4,128)S(1)}, f32[3,1024]{1,0:T(4,128)S(1)}) fusion(bf16[1024,3,1024]{2,0,1:T(8,128)(2,1)} %param.16, f32[1024]{0:T(1024)S(1)} %bitcast.76, f32[1024]{0:T(1024)S(1)} %bitcast.75), kind=kLoop, calls=%fused_computation.2 | loop fusion | flops 15722496 | bytes 6324224 | tf_op jit(solution)/shard_map/reduce_sum | solution.py:311
  5.9 5.1 %collective-permute-start.4 = (f32[2,3,1024]{2,1,0:T(4,128)S(1)}, f32[2,3,1024]{2,1,0:T(4,128)S(1)}, u32[]{:S(2)}, u32[]{:S(2)}) collective-permute-start(f32[2,3,1024]{2,1,0:T(4,128)S(1)} %pad_maximum_fusion.11), channel_id=1, source_target_pairs={{0,12},{4,0},{8,4},{12,8},{1,13},{5,1},{9,5},{13,9},{2,14},{6,2},{... | collective-permute-start | bytes 73736 | tf_op jit(solution)/shard_map/ppermute | solution.py:301
  12.0 1.5 collective-permute-start.15
  15.2 1.8 sine_multiply_fusion.1
  18.3 1.5 collective-permute-start.10
  19.9 7.0 %collective-permute-done.15 = bf16[256,1024]{1,0:T(8,128)(2,1)} collective-permute-done((bf16[256,1024]{1,0:T(8,128)(2,1)S(1)}, bf16[256,1024]{1,0:T(8,128)(2,1)}, u32[]{:S(2)}, u32[]{:S(2)}) %collective-permute-start.15) | collective-permute-done | bytes 524320 | tf_op jit(solution)/shard_map/ppermute | solution.py:292
  28.2 10.0 %collective-permute-done = bf16[256,1024]{1,0:T(8,128)(2,1)} collective-permute-done((bf16[256,1024]{1,0:T(8,128)(2,1)S(1)}, bf16[256,1024]{1,0:T(8,128)(2,1)}, u32[]{:S(2)}, u32[]{:S(2)}) %collective-permute-start) | collective-permute-done | bytes 524320 | tf_op jit(solution)/shard_map/ppermute | solution.py:292
  40.2 1.6 collective-permute-start.5
  42.9 5.1 %collective-permute-done.5 = f32[6,1024]{1,0:T(8,128)S(1)} collective-permute-done((f32[6,1024]{1,0:T(8,128)S(1)}, f32[6,1024]{1,0:T(8,128)S(1)}, u32[]{:S(2)}, u32[]{:S(2)}) %collective-permute-start.5) | collective-permute-done | bytes 24608 | tf_op jit(solution)/shard_map/ppermute | solution.py:292
  48.1 1.3 pad_maximum_fusion.1.my_ref
  50.7 8.8 %shard_map.129 = bf16[4,256,256]{2,1,0:T(8,128)(2,1)} custom-call(s32[4]{0:T(128)} %pad_add_fusion.order, bf16[2,256,1024]{2,1,0:T(8,128)(2,1)} %copy-done.4, bf16[2,256,1024]{2,1,0:T(8,128)(2,1)} %collective-permute-done.16.other_ref, f32[4,3,1024]{2,1,0:T(4,128)} %get-tuple-element.45.mods_ref, bf16[4096,512]{1,0:T(8,128)(2,1)} %refs_3_.6, ...), custom_call_target="tpu_custom_call" | custom-call | flops 2147483648 | bytes 8388608 | tf_op jit(solution)/shard_map/pallas_call | solution.py:100
  59.5 1.1 constant_dynamic-slice_fusion.3
  60.6 3.1 %collective-permute-start.19 = (bf16[1,256,256]{2,1,0:T(8,128)(2,1)S(1)}, bf16[1,256,256]{2,1,0:T(8,128)(2,1)S(1)}, u32[]{:S(2)}, u32[]{:S(2)}) collective-permute-start(bf16[1,256,256]{2,1,0:T(8,128)(2,1)S(1)} %get-tuple-element.26), channel_id=1, source_target_pairs={{0,12},{4,0},{8,4},{12,8},{1,13},{5,1},{9,5},{13,9},{2,14},{6,2},{... | collective-permute-start | bytes 393224 | tf_op jit(solution)/shard_map/ppermute | solution.py:301
  64.9 10.5 %shard_map.127 = bf16[4,256,384]{2,1,0:T(8,128)(2,1)} custom-call(s32[4]{0:T(128)} %pad_add_fusion.order, bf16[2,256,1024]{2,1,0:T(8,128)(2,1)} %copy-done.1, bf16[2,256,1024]{2,1,0:T(8,128)(2,1)} %collective-permute-done.1.other_ref, f32[4,3,1024]{2,1,0:T(4,128)} %get-tuple-element.46.mods_ref, bf16[4096,512]{1,0:T(8,128)(2,1)} %refs_3_.5, ...), custom_call_target="tpu_custom_call" | custom-call | flops 3221225472 | bytes 12582912 | tf_op jit(solution)/shard_map/pallas_call | solution.py:100
  75.4 1.3 constant_dynamic-slice_fusion.11
  76.7 3.8 %collective-permute-start.9 = (bf16[1,256,384]{2,1,0:T(8,128)(2,1)S(1)}, bf16[1,256,384]{2,1,0:T(8,128)(2,1)S(1)}, u32[]{:S(2)}, u32[]{:S(2)}) collective-permute-start(bf16[1,256,384]{2,1,0:T(8,128)(2,1)S(1)} %get-tuple-element.18), channel_id=1, source_target_pairs={{0,12},{4,0},{8,4},{12,8},{1,13},{5,1},{9,5},{13,9},{2,14},{6,2},{... | collective-permute-start | bytes 589832 | tf_op jit(solution)/shard_map/ppermute | solution.py:301
  80.8 10.5 %shard_map.128 = bf16[4,256,384]{2,1,0:T(8,128)(2,1)} custom-call(s32[4]{0:T(128)} %pad_add_fusion.order, bf16[2,256,1024]{2,1,0:T(8,128)(2,1)} %copy-done.2, bf16[2,256,1024]{2,1,0:T(8,128)(2,1)} %collective-permute-done.11.other_ref, f32[4,3,1024]{2,1,0:T(4,128)} %get-tuple-element.46.mods_ref, bf16[4096,512]{1,0:T(8,128)(2,1)} %refs_3_.5, ...), custom_call_target="tpu_custom_call" | custom-call | flops 3221225472 | bytes 12582912 | tf_op jit(solution)/shard_map/pallas_call | solution.py:100
  91.7 1.3 constant_dynamic-slice_fusion.7
  93.0 3.5 %collective-permute-start.14 = (bf16[1,256,384]{2,1,0:T(8,128)(2,1)S(1)}, bf16[1,256,384]{2,1,0:T(8,128)(2,1)S(1)}, u32[]{:S(2)}, u32[]{:S(2)}) collective-permute-start(bf16[1,256,384]{2,1,0:T(8,128)(2,1)S(1)} %get-tuple-element.22), channel_id=1, source_target_pairs={{0,12},{4,0},{8,4},{12,8},{1,13},{5,1},{9,5},{13,9},{2,14},{6,2},{... | collective-permute-start | bytes 589832 | tf_op jit(solution)/shard_map/ppermute | solution.py:301
  98.3 2.7 %collective-permute-done.7 = bf16[1,256,384]{2,1,0:T(8,128)(2,1)S(1)} collective-permute-done((bf16[1,256,384]{2,1,0:T(8,128)(2,1)S(1)}, bf16[1,256,384]{2,1,0:T(8,128)(2,1)S(1)}, u32[]{:S(2)}, u32[]{:S(2)}) %collective-permute-start.7) | collective-permute-done | bytes 196640 | tf_op jit(solution)/shard_map/ppermute | solution.py:301
  101.9 13.8 %shard_map.130 = (f32[1,2048,128]{2,1,0:T(8,128)}, f32[1,2048,128]{2,1,0:T(8,128)}, f32[1,2048,128]{2,1,0:T(8,128)}) custom-call(f32[1]{0:T(128)} %dynamic_slice.64.lam_ref, bf16[1,1024,384]{2,1,0:T(8,128)(2,1)} %pad_maximum_fusion.4.refs_0_.refs_3_.refs_4_, bf16[1,1024,256]{2,1,0:T(8,128)(2,1)} %pad_maximum_fusion.6.refs_1_.refs_2_, ...), custom_call_target="tpu_custom_call" | custom-call | flops 3221225472 | bytes 1048576 | tf_op jit(solution)/shard_map/pallas_call | solution.py:223
  116.6 10.4 %shard_map.131.refs_8_ = bf16[1,1024,128]{2,1,0:T(8,128)(2,1)} custom-call(f32[1]{0:T(128)} %dynamic_slice.64.lam_ref, bf16[1,1024,384]{2,1,0:T(8,128)(2,1)} %pad_maximum_fusion.4.refs_0_.refs_3_.refs_4_, bf16[1,1024,384]{2,1,0:T(8,128)(2,1)} %pad_maximum_fusion.5.refs_1_.refs_2_.refs_0_.refs_5_.refs_6_, ...), custom_call_target="tpu_custom_call" | custom-call | flops 1610612736 | bytes 524288 | tf_op jit(solution)/shard_map/pallas_call | solution.py:223
  127.0 20.0 %shard_map.132 = bf16[1,1024,128]{2,1,0:T(8,128)(2,1)} custom-call(f32[1]{0:T(128)} %dynamic_slice.64.lam_ref, bf16[1,1024,384]{2,1,0:T(8,128)(2,1)} %pad_maximum_fusion.5.refs_1_.refs_2_.refs_0_.refs_5_.refs_6_, bf16[1,1024,256]{2,1,0:T(8,128)(2,1)} %pad_maximum_fusion.6.refs_1_.refs_2_, bf16[1,1024,256]{2,1,0:T(8,128)(2,1)} %pad_maximum_fusion.6.refs_1_.refs_2_, ...), custom_call_target="tpu_custom_call" | custom-call | flops 4831838208 | bytes 1572864 | tf_op jit(solution)/shard_map/pallas_call | solution.py:223
  148.0 6.9 %collective-permute-start.25 = (bf16[1,256,128]{2,1,0:T(8,128)(2,1)S(1)}, bf16[1,256,128]{2,1,0:T(8,128)(2,1)S(1)}, u32[]{:S(2)}, u32[]{:S(2)}) collective-permute-start(bf16[1,256,128]{2,1,0:T(8,128)(2,1)S(1)} %get-tuple-element.42), channel_id=1, source_target_pairs={{0,4},{4,8},{8,12},{12,0},{1,5},{5,9},{9,13},{13,1},{2,6},{6,10},{... | collective-permute-start | bytes 196616 | tf_op jit(solution)/shard_map/ppermute | solution.py:301
  154.9 2.1 %collective-permute-start.24 = (bf16[1,256,128]{2,1,0:T(8,128)(2,1)S(1)}, bf16[1,256,128]{2,1,0:T(8,128)(2,1)S(1)}, u32[]{:S(2)}, u32[]{:S(2)}) collective-permute-start(bf16[1,256,128]{2,1,0:T(8,128)(2,1)S(1)} %get-tuple-element.43), channel_id=1, source_target_pairs={{0,8},{4,12},{8,0},{12,4},{1,9},{5,13},{9,1},{13,5},{2,10},{6,14},... | collective-permute-start | bytes 196616 | tf_op jit(solution)/shard_map/ppermute | solution.py:301
  157.0 2.8 %collective-permute-start.23 = (bf16[1,256,128]{2,1,0:T(8,128)(2,1)S(1)}, bf16[1,256,128]{2,1,0:T(8,128)(2,1)S(1)}, u32[]{:S(2)}, u32[]{:S(2)}) collective-permute-start(bf16[1,256,128]{2,1,0:T(8,128)(2,1)S(1)} %get-tuple-element.44), channel_id=1, source_target_pairs={{0,12},{4,0},{8,4},{12,8},{1,13},{5,1},{9,5},{13,9},{2,14},{6,2},{... | collective-permute-start | bytes 196616 | tf_op jit(solution)/shard_map/ppermute | solution.py:301
  160.5 3.3 %collective-permute-start.20 = (bf16[1,256,128]{2,1,0:T(8,128)(2,1)S(1)}, bf16[1,256,128]{2,1,0:T(8,128)(2,1)S(1)}, u32[]{:S(2)}, u32[]{:S(2)}) collective-permute-start(bf16[1,256,128]{2,1,0:T(8,128)(2,1)S(1)} %get-tuple-element.36), channel_id=1, source_target_pairs={{0,12},{4,0},{8,4},{12,8},{1,13},{5,1},{9,5},{13,9},{2,14},{6,2},{... | collective-permute-start | bytes 196616 | tf_op jit(solution)/shard_map/ppermute | solution.py:301
  163.8 2.2 %collective-permute-done.22 = bf16[1,256,128]{2,1,0:T(8,128)(2,1)S(1)} collective-permute-done((bf16[1,256,128]{2,1,0:T(8,128)(2,1)S(1)}, bf16[1,256,128]{2,1,0:T(8,128)(2,1)S(1)}, u32[]{:S(2)}, u32[]{:S(2)}) %collective-permute-start.22) | collective-permute-done | bytes 65568 | tf_op jit(solution)/shard_map/ppermute | solution.py:301
  166.9 1.5 collective-permute-start.26
  168.5 7.6 %collective-permute-done.26 = bf16[512,512]{1,0:T(8,128)(2,1)S(1)} collective-permute-done((bf16[512,512]{1,0:T(8,128)(2,1)S(1)}, bf16[512,512]{1,0:T(8,128)(2,1)S(1)}, u32[]{:S(2)}, u32[]{:S(2)}) %collective-permute-start.26) | collective-permute-done | bytes 524320 | tf_op jit(solution)/shard_map/ppermute | solution.py:292
  176.3 2.6 %collective-permute-done.27.other_ref = bf16[2,512,512]{2,1,0:T(8,128)(2,1)S(1)} collective-permute-done((bf16[2,512,512]{2,1,0:T(8,128)(2,1)S(1)}, bf16[2,512,512]{2,1,0:T(8,128)(2,1)S(1)}, u32[]{:S(2)}, u32[]{:S(2)}) %collective-permute-start.27) | collective-permute-done | bytes 1048608 | tf_op jit(solution)/shard_map/ppermute | solution.py:298
  180.0 7.3 %shard_map.133 = bf16[512,1024]{1,0:T(8,128)(2,1)} custom-call(s32[4]{0:T(128)} %pad_add_fusion.order, bf16[2,512,512]{2,1,0:T(8,128)(2,1)} %copy-done.3, bf16[2,512,512]{2,1,0:T(8,128)(2,1)} %copy-done.5, bf16[512,1024]{1,0:T(8,128)(2,1)} %lat_ref.1, f32[1,1024]{1,0:T(1,128)} %get-tuple-element.47.gate_ref, bf16[2048,1024]{1,0:T(8,128)(2,1)} %refs_3_.7, ...), custom_call_target="tpu_custom_call" | custom-call | tf_op jit(solution)/shard_map/pallas_call | solution.py:258
  (94 shorter events, 19.6 us)
Async XLA Ops:
  5.9 12.5 %collective-permute-start.4 = (f32[2,3,1024]{2,1,0:T(4,128)S(1)}, f32[2,3,1024]{2,1,0:T(4,128)S(1)}, u32[]{:S(2)}, u32[]{:S(2)}) collective-permute-start(f32[2,3,1024]{2,1,0:T(4,128)S(1)} %pad_maximum_fusion.11), channel_id=1, source_target_pairs={{0,12},{4,0},{8,4},{12,8},{1,13},{5,1},{9,5},{13,9},{2,14},{6,2},{... | collective-permute-start | bytes 73736 | tf_op jit(solution)/shard_map/ppermute | solution.py:301
  11.0 8.8 %collective-permute-start.3 = (f32[2,3,1024]{2,1,0:T(4,128)S(1)}, f32[2,3,1024]{2,1,0:T(4,128)S(1)}, u32[]{:S(2)}, u32[]{:S(2)}) collective-permute-start(f32[2,3,1024]{2,1,0:T(4,128)S(1)} %pad_maximum_fusion.11), channel_id=1, source_target_pairs={{0,8},{4,12},{8,0},{12,4},{1,9},{5,13},{9,1},{13,5},{2,10},{6,14},... | collective-permute-start | bytes 73736 | tf_op jit(solution)/shard_map/ppermute | solution.py:301
  11.0 8.8 %collective-permute-start.2 = (f32[2,3,1024]{2,1,0:T(4,128)S(1)}, f32[2,3,1024]{2,1,0:T(4,128)S(1)}, u32[]{:S(2)}, u32[]{:S(2)}) collective-permute-start(f32[2,3,1024]{2,1,0:T(4,128)S(1)} %pad_maximum_fusion.11), channel_id=1, source_target_pairs={{0,4},{4,8},{8,12},{12,0},{1,5},{5,9},{9,13},{13,1},{2,6},{6,10},{... | collective-permute-start | bytes 73736 | tf_op jit(solution)/shard_map/ppermute | solution.py:301
  12.0 14.9 %collective-permute-start.15 = (bf16[256,1024]{1,0:T(8,128)(2,1)S(1)}, bf16[256,1024]{1,0:T(8,128)(2,1)}, u32[]{:S(2)}, u32[]{:S(2)}) collective-permute-start(bf16[256,1024]{1,0:T(8,128)(2,1)S(1)} %copy-done.6), channel_id=1, source_target_pairs={{0,2},{1,3},{2,0},{3,1},{4,6},{5,7},{6,4},{7,5},{8,10},{9,11},{10,... | collective-permute-start | bytes 1572872 | tf_op jit(solution)/shard_map/ppermute | solution.py:292
  14.6 23.5 %collective-permute-start = (bf16[256,1024]{1,0:T(8,128)(2,1)S(1)}, bf16[256,1024]{1,0:T(8,128)(2,1)}, u32[]{:S(2)}, u32[]{:S(2)}) collective-permute-start(bf16[256,1024]{1,0:T(8,128)(2,1)S(1)} %get-tuple-element.15), channel_id=1, source_target_pairs={{0,2},{1,3},{2,0},{3,1},{4,6},{5,7},{6,4},{7,5},{8,10},{9,11},{10,... | collective-permute-start | bytes 1572872 | tf_op jit(solution)/shard_map/ppermute | solution.py:292
  18.3 29.8 %collective-permute-start.10 = (bf16[256,1024]{1,0:T(8,128)(2,1)S(1)}, bf16[256,1024]{1,0:T(8,128)(2,1)}, u32[]{:S(2)}, u32[]{:S(2)}) collective-permute-start(bf16[256,1024]{1,0:T(8,128)(2,1)S(1)} %get-tuple-element.16), channel_id=1, source_target_pairs={{0,2},{1,3},{2,0},{3,1},{4,6},{5,7},{6,4},{7,5},{8,10},{9,11},{10,... | collective-permute-start | bytes 1572872 | tf_op jit(solution)/shard_map/ppermute | solution.py:292
  28.0 21.4 %copy-start.4 = (bf16[2,256,1024]{2,1,0:T(8,128)(2,1)}, bf16[2,256,1024]{2,1,0:T(8,128)(2,1)S(1)}, u32[]{:S(2)}) copy-start(bf16[2,256,1024]{2,1,0:T(8,128)(2,1)S(1)} %pad_maximum_fusion.2.my_ref) | copy-start | bytes 3145732
  28.1 14.2 %copy-start.11 = (f32[4]{0:T(128)S(1)}, f32[4]{0:T(128)}, u32[]{:S(2)}) copy-start(f32[4]{0:T(128)} %param.23) | copy-start | bytes 52
  28.1 22.6 %collective-permute-start.16 = (bf16[2,256,1024]{2,1,0:T(8,128)(2,1)S(1)}, bf16[2,256,1024]{2,1,0:T(8,128)(2,1)}, u32[]{:S(2)}, u32[]{:S(2)}) collective-permute-start(bf16[2,256,1024]{2,1,0:T(8,128)(2,1)S(1)} %pad_maximum_fusion.2.my_ref), channel_id=1, source_target_pairs={{0,1},{1,0},{2,3},{3,2},{4,5},{5,4},{6,7},{7,6},{8,9},{9,8},{10,11... | collective-permute-start | bytes 3145736 | tf_op jit(solution)/shard_map/ppermute | solution.py:298
  39.3 20.2 %copy-start.1 = (bf16[2,256,1024]{2,1,0:T(8,128)(2,1)}, bf16[2,256,1024]{2,1,0:T(8,128)(2,1)S(1)}, u32[]{:S(2)}) copy-start(bf16[2,256,1024]{2,1,0:T(8,128)(2,1)S(1)} %pad_maximum_fusion.my_ref) | copy-start | bytes 3145732
  39.3 25.6 %collective-permute-start.1 = (bf16[2,256,1024]{2,1,0:T(8,128)(2,1)S(1)}, bf16[2,256,1024]{2,1,0:T(8,128)(2,1)}, u32[]{:S(2)}, u32[]{:S(2)}) collective-permute-start(bf16[2,256,1024]{2,1,0:T(8,128)(2,1)S(1)} %pad_maximum_fusion.my_ref), channel_id=1, source_target_pairs={{0,1},{1,0},{2,3},{3,2},{4,5},{5,4},{6,7},{7,6},{8,9},{9,8},{10,11... | collective-permute-start | bytes 3145736 | tf_op jit(solution)/shard_map/ppermute | solution.py:298
  40.2 7.8 %collective-permute-start.5 = (f32[6,1024]{1,0:T(8,128)S(1)}, f32[6,1024]{1,0:T(8,128)S(1)}, u32[]{:S(2)}, u32[]{:S(2)}) collective-permute-start(f32[6,1024]{1,0:T(8,128)S(1)} %concatenate.38), channel_id=1, source_target_pairs={{0,2},{1,3},{2,0},{3,1},{4,6},{5,7},{6,4},{7,5},{8,10},{9,11},{10,... | collective-permute-start | bytes 73736 | tf_op jit(solution)/shard_map/ppermute | solution.py:292
  48.0 2.0 %collective-permute-start.6 = (f32[2,6,1024]{2,1,0:T(8,128)S(1)}, f32[2,6,1024]{2,1,0:T(8,128)S(1)}, u32[]{:S(2)}, u32[]{:S(2)}) collective-permute-start(f32[2,6,1024]{2,1,0:T(8,128)S(1)} %pad_maximum_fusion.10), channel_id=1, source_target_pairs={{0,1},{1,0},{2,3},{3,2},{4,5},{5,4},{6,7},{7,6},{8,9},{9,8},{10,11... | collective-permute-start | bytes 147464 | tf_op jit(solution)/shard_map/ppermute | solution.py:298
  49.4 31.1 %collective-permute-start.11 = (bf16[2,256,1024]{2,1,0:T(8,128)(2,1)S(1)}, bf16[2,256,1024]{2,1,0:T(8,128)(2,1)}, u32[]{:S(2)}, u32[]{:S(2)}) collective-permute-start(bf16[2,256,1024]{2,1,0:T(8,128)(2,1)S(1)} %pad_maximum_fusion.1.my_ref), channel_id=1, source_target_pairs={{0,1},{1,0},{2,3},{3,2},{4,5},{5,4},{6,7},{7,6},{8,9},{9,8},{10,11... | collective-permute-start | bytes 3145736 | tf_op jit(solution)/shard_map/ppermute | solution.py:298
  60.6 30.7 %collective-permute-start.19 = (bf16[1,256,256]{2,1,0:T(8,128)(2,1)S(1)}, bf16[1,256,256]{2,1,0:T(8,128)(2,1)S(1)}, u32[]{:S(2)}, u32[]{:S(2)}) collective-permute-start(bf16[1,256,256]{2,1,0:T(8,128)(2,1)S(1)} %get-tuple-element.26), channel_id=1, source_target_pairs={{0,12},{4,0},{8,4},{12,8},{1,13},{5,1},{9,5},{13,9},{2,14},{6,2},{... | collective-permute-start | bytes 393224 | tf_op jit(solution)/shard_map/ppermute | solution.py:301
  63.7 29.3 %collective-permute-start.18 = (bf16[1,256,256]{2,1,0:T(8,128)(2,1)S(1)}, bf16[1,256,256]{2,1,0:T(8,128)(2,1)S(1)}, u32[]{:S(2)}, u32[]{:S(2)}) collective-permute-start(bf16[1,256,256]{2,1,0:T(8,128)(2,1)S(1)} %get-tuple-element.27), channel_id=1, source_target_pairs={{0,8},{4,12},{8,0},{12,4},{1,9},{5,13},{9,1},{13,5},{2,10},{6,14},... | collective-permute-start | bytes 393224 | tf_op jit(solution)/shard_map/ppermute | solution.py:301
  64.6 32.0 %collective-permute-start.17 = (bf16[1,256,256]{2,1,0:T(8,128)(2,1)S(1)}, bf16[1,256,256]{2,1,0:T(8,128)(2,1)S(1)}, u32[]{:S(2)}, u32[]{:S(2)}) collective-permute-start(bf16[1,256,256]{2,1,0:T(8,128)(2,1)S(1)} %get-tuple-element.28), channel_id=1, source_target_pairs={{0,4},{4,8},{8,12},{12,0},{1,5},{5,9},{9,13},{13,1},{2,6},{6,10},{... | collective-permute-start | bytes 393224 | tf_op jit(solution)/shard_map/ppermute | solution.py:301
  76.7 21.5 %collective-permute-start.9 = (bf16[1,256,384]{2,1,0:T(8,128)(2,1)S(1)}, bf16[1,256,384]{2,1,0:T(8,128)(2,1)S(1)}, u32[]{:S(2)}, u32[]{:S(2)}) collective-permute-start(bf16[1,256,384]{2,1,0:T(8,128)(2,1)S(1)} %get-tuple-element.18), channel_id=1, source_target_pairs={{0,12},{4,0},{8,4},{12,8},{1,13},{5,1},{9,5},{13,9},{2,14},{6,2},{... | collective-permute-start | bytes 589832 | tf_op jit(solution)/shard_map/ppermute | solution.py:301
  80.5 17.8 %collective-permute-start.8 = (bf16[1,256,384]{2,1,0:T(8,128)(2,1)S(1)}, bf16[1,256,384]{2,1,0:T(8,128)(2,1)S(1)}, u32[]{:S(2)}, u32[]{:S(2)}) collective-permute-start(bf16[1,256,384]{2,1,0:T(8,128)(2,1)S(1)} %get-tuple-element.19), channel_id=1, source_target_pairs={{0,8},{4,12},{8,0},{12,4},{1,9},{5,13},{9,1},{13,5},{2,10},{6,14},... | collective-permute-start | bytes 589832 | tf_op jit(solution)/shard_map/ppermute | solution.py:301
  91.3 9.6 %collective-permute-start.7 = (bf16[1,256,384]{2,1,0:T(8,128)(2,1)S(1)}, bf16[1,256,384]{2,1,0:T(8,128)(2,1)S(1)}, u32[]{:S(2)}, u32[]{:S(2)}) collective-permute-start(bf16[1,256,384]{2,1,0:T(8,128)(2,1)S(1)} %get-tuple-element.20), channel_id=1, source_target_pairs={{0,4},{4,8},{8,12},{12,0},{1,5},{5,9},{9,13},{13,1},{2,6},{6,10},{... | collective-permute-start | bytes 589832 | tf_op jit(solution)/shard_map/ppermute | solution.py:301
  93.0 22.6 %collective-permute-start.14 = (bf16[1,256,384]{2,1,0:T(8,128)(2,1)S(1)}, bf16[1,256,384]{2,1,0:T(8,128)(2,1)S(1)}, u32[]{:S(2)}, u32[]{:S(2)}) collective-permute-start(bf16[1,256,384]{2,1,0:T(8,128)(2,1)S(1)} %get-tuple-element.22), channel_id=1, source_target_pairs={{0,12},{4,0},{8,4},{12,8},{1,13},{5,1},{9,5},{13,9},{2,14},{6,2},{... | collective-permute-start | bytes 589832 | tf_op jit(solution)/shard_map/ppermute | solution.py:301
  96.5 19.1 %collective-permute-start.13 = (bf16[1,256,384]{2,1,0:T(8,128)(2,1)S(1)}, bf16[1,256,384]{2,1,0:T(8,128)(2,1)S(1)}, u32[]{:S(2)}, u32[]{:S(2)}) collective-permute-start(bf16[1,256,384]{2,1,0:T(8,128)(2,1)S(1)} %get-tuple-element.23), channel_id=1, source_target_pairs={{0,8},{4,12},{8,0},{12,4},{1,9},{5,13},{9,1},{13,5},{2,10},{6,14},... | collective-permute-start | bytes 589832 | tf_op jit(solution)/shard_map/ppermute | solution.py:301
  98.2 17.4 %collective-permute-start.12 = (bf16[1,256,384]{2,1,0:T(8,128)(2,1)S(1)}, bf16[1,256,384]{2,1,0:T(8,128)(2,1)S(1)}, u32[]{:S(2)}, u32[]{:S(2)}) collective-permute-start(bf16[1,256,384]{2,1,0:T(8,128)(2,1)S(1)} %get-tuple-element.24), channel_id=1, source_target_pairs={{0,4},{4,8},{8,12},{12,0},{1,5},{5,9},{9,13},{13,1},{2,6},{6,10},{... | collective-permute-start | bytes 589832 | tf_op jit(solution)/shard_map/ppermute | solution.py:301
  127.0 32.9 %copy-start.7 = (bf16[1,1024,128]{2,1,0:T(8,128)(2,1)S(1)}, bf16[1,1024,128]{2,1,0:T(8,128)(2,1)}, u32[]{:S(2)}) copy-start(bf16[1,1024,128]{2,1,0:T(8,128)(2,1)} %shard_map.131.refs_8_) | copy-start | bytes 786436
  148.0 12.5 %collective-permute-start.25 = (bf16[1,256,128]{2,1,0:T(8,128)(2,1)S(1)}, bf16[1,256,128]{2,1,0:T(8,128)(2,1)S(1)}, u32[]{:S(2)}, u32[]{:S(2)}) collective-permute-start(bf16[1,256,128]{2,1,0:T(8,128)(2,1)S(1)} %get-tuple-element.42), channel_id=1, source_target_pairs={{0,4},{4,8},{8,12},{12,0},{1,5},{5,9},{9,13},{13,1},{2,6},{6,10},{... | collective-permute-start | bytes 196616 | tf_op jit(solution)/shard_map/ppermute | solution.py:301
  154.9 8.9 %collective-permute-start.24 = (bf16[1,256,128]{2,1,0:T(8,128)(2,1)S(1)}, bf16[1,256,128]{2,1,0:T(8,128)(2,1)S(1)}, u32[]{:S(2)}, u32[]{:S(2)}) collective-permute-start(bf16[1,256,128]{2,1,0:T(8,128)(2,1)S(1)} %get-tuple-element.43), channel_id=1, source_target_pairs={{0,8},{4,12},{8,0},{12,4},{1,9},{5,13},{9,1},{13,5},{2,10},{6,14},... | collective-permute-start | bytes 196616 | tf_op jit(solution)/shard_map/ppermute | solution.py:301
  157.0 6.8 %collective-permute-start.23 = (bf16[1,256,128]{2,1,0:T(8,128)(2,1)S(1)}, bf16[1,256,128]{2,1,0:T(8,128)(2,1)S(1)}, u32[]{:S(2)}, u32[]{:S(2)}) collective-permute-start(bf16[1,256,128]{2,1,0:T(8,128)(2,1)S(1)} %get-tuple-element.44), channel_id=1, source_target_pairs={{0,12},{4,0},{8,4},{12,8},{1,13},{5,1},{9,5},{13,9},{2,14},{6,2},{... | collective-permute-start | bytes 196616 | tf_op jit(solution)/shard_map/ppermute | solution.py:301
  159.9 6.1 %collective-permute-start.22 = (bf16[1,256,128]{2,1,0:T(8,128)(2,1)S(1)}, bf16[1,256,128]{2,1,0:T(8,128)(2,1)S(1)}, u32[]{:S(2)}, u32[]{:S(2)}) collective-permute-start(bf16[1,256,128]{2,1,0:T(8,128)(2,1)S(1)} %get-tuple-element.34), channel_id=1, source_target_pairs={{0,4},{4,8},{8,12},{12,0},{1,5},{5,9},{9,13},{13,1},{2,6},{6,10},{... | collective-permute-start | bytes 196616 | tf_op jit(solution)/shard_map/ppermute | solution.py:301
  160.0 6.1 %collective-permute-start.21 = (bf16[1,256,128]{2,1,0:T(8,128)(2,1)S(1)}, bf16[1,256,128]{2,1,0:T(8,128)(2,1)S(1)}, u32[]{:S(2)}, u32[]{:S(2)}) collective-permute-start(bf16[1,256,128]{2,1,0:T(8,128)(2,1)S(1)} %get-tuple-element.35), channel_id=1, source_target_pairs={{0,8},{4,12},{8,0},{12,4},{1,9},{5,13},{9,1},{13,5},{2,10},{6,14},... | collective-permute-start | bytes 196616 | tf_op jit(solution)/shard_map/ppermute | solution.py:301
  160.5 6.2 %collective-permute-start.20 = (bf16[1,256,128]{2,1,0:T(8,128)(2,1)S(1)}, bf16[1,256,128]{2,1,0:T(8,128)(2,1)S(1)}, u32[]{:S(2)}, u32[]{:S(2)}) collective-permute-start(bf16[1,256,128]{2,1,0:T(8,128)(2,1)S(1)} %get-tuple-element.36), channel_id=1, source_target_pairs={{0,12},{4,0},{8,4},{12,8},{1,13},{5,1},{9,5},{13,9},{2,14},{6,2},{... | collective-permute-start | bytes 196616 | tf_op jit(solution)/shard_map/ppermute | solution.py:301
  166.9 9.2 %collective-permute-start.26 = (bf16[512,512]{1,0:T(8,128)(2,1)S(1)}, bf16[512,512]{1,0:T(8,128)(2,1)S(1)}, u32[]{:S(2)}, u32[]{:S(2)}) collective-permute-start(bf16[512,512]{1,0:T(8,128)(2,1)S(1)} %maximum_maximum_fusion), channel_id=1, source_target_pairs={{0,2},{1,3},{2,0},{3,1},{4,6},{5,7},{6,4},{7,5},{8,10},{9,11},{10,... | collective-permute-start | bytes 1572872 | tf_op jit(solution)/shard_map/ppermute | solution.py:292
  176.3 2.7 %collective-permute-start.27 = (bf16[2,512,512]{2,1,0:T(8,128)(2,1)S(1)}, bf16[2,512,512]{2,1,0:T(8,128)(2,1)S(1)}, u32[]{:S(2)}, u32[]{:S(2)}) collective-permute-start(bf16[2,512,512]{2,1,0:T(8,128)(2,1)S(1)} %pad_maximum_fusion.3.my_ref), channel_id=1, source_target_pairs={{0,1},{1,0},{2,3},{3,2},{4,5},{5,4},{6,7},{7,6},{8,9},{9,8},{10,11... | collective-permute-start | bytes 3145736 | tf_op jit(solution)/shard_map/ppermute | solution.py:298
  (8 other events, 73.0 us)
